TPU v7x, 256 devices: a whole 4x4x8 slice. The times are simulated.
256 devices in a mesh: ep: 64 (over z, x, core), tp: 4 (over y).
Axes of the slice: x: 4, y: 4, z: 8, core: 2. Of those that a mesh axis runs over, the one named last changes fastest.
Arguments:
- queries: bfloat16 [16384, 2, 1024], P('ep', None, 'tp')
- keys: bfloat16 [16384, 2, 256], P('ep', None, 'tp')
- values: bfloat16 [16384, 2, 256], P('ep', None, 'tp'), may hold values from -6 to 6
- query_gain: float32 [64], replicated, may hold values from 1.2 to 6
- key_gain: float32 [64], replicated, may hold values from 1.2 to 6
- out_weight: bfloat16 [1024, 2048], P('tp'), may hold values from -0.75 to 0.75
- moe_tokens: bfloat16 [32768, 2048], P(('ep', 'tp')), may hold values from -6 to 6
- moe_gain: float32 [2048], replicated, may hold values from 0.1 to 1.9
- routes: int32 [32768, 2], P(('ep', 'tp')), may hold values from 0 to 63, all different within a row; in each aligned block of 128 rows (0 to 127, 128 to 255, ...) at most 6 rows name the same one
- route_weight: float32 [32768, 2], P(('ep', 'tp')), may hold values from 0.1 to 1
- w_gate: bfloat16 [64, 2048, 1024], P('ep', None, 'tp'), may hold values from -0.125 to 0.125
- w_up: bfloat16 [64, 2048, 1024], P('ep', None, 'tp'), may hold values from -0.125 to 0.125
- w_down: bfloat16 [64, 1024, 2048], P('ep', 'tp'), may hold values from -0.1875 to 0.1875
Outputs:
- attended: bfloat16 [16384, 2, 2048], P(('ep', 'tp'))
- routed: bfloat16 [32768, 2048], P(('ep', 'tp'))
Inputs may be any that keep to these rules, and one draw needn't show every extreme that they name: `routes`: each row names 2 different experts. The rows of one device name no expert more than 6 times, and in every draw some device's rows name one expert exactly 6 times.
All inputs are finite; a program needn't handle non-finite values.
Results may differ from a plain program's by a relative error of at most 0.013.
The roundings to bfloat16 on the way count: a program that leaves them out, or rounds other values in their place, can miss the bound.
Values may be sent and summed in bfloat16 or wider, within the bound.
A program may use at most 128 MiB of HBM per device.

v0:
```python
import math

import jax
import jax.numpy as jnp
from jax import lax
from jax.sharding import PartitionSpec as P

HEAD_DIM = 64
GRID_W = 64


EPS = 1e-06
THETA = 10000.0


def in_one_piece(arrays, axis, dim, along):
    ends, at = ([], 0)
    for a in arrays[:-1]:
        at += a.shape[along]
        ends.append(at)
    both = jnp.concatenate(arrays, axis=along)
    return tuple(jnp.split(lax.all_gather(both, axis, axis=dim, tiled=True), ends, axis=along))


def in_blocks(value, dim, size):
    lengths = value.shape
    tiles = value.reshape(*lengths[:dim], size, lengths[dim] // size, *lengths[dim + 1 :])
    return jnp.moveaxis(tiles, dim, 0)


def sum_at_owner(value, axis, dim):
    tiles = in_blocks(value, dim, lax.axis_size(axis))
    arrived = lax.all_to_all(tiles, axis, split_axis=0, concat_axis=0, tiled=True)
    return arrived.astype(jnp.float32).sum(axis=0)


def in_order(tiles, dim):
    lengths = list(tiles.shape[1:])
    lengths[dim] *= tiles.shape[0]
    return jnp.moveaxis(tiles, 0, dim).reshape(lengths)


def work_in_pieces(value, axis, dim, work, out_dim):
    span = value.shape[dim]
    pieces = jnp.split(value, 2, axis=dim) if span % 2 == 0 else [value]
    initial = jnp.arange(lax.axis_size(axis)) * span
    tiles = [lax.all_gather(piece, axis) for piece in pieces]
    made = [jax.vmap(work)(b, initial + k * (span // len(pieces))) for k, b in enumerate(tiles)]
    return in_order(jnp.concatenate(made, axis=out_dim + 1), out_dim)


def turn(normed, positions):
    quarter = normed.shape[-1] // 4
    inverse = THETA ** (-jnp.arange(quarter, dtype=jnp.float32) / quarter)
    grid_row = (positions // GRID_W).astype(jnp.float32)
    grid_col = (positions % GRID_W).astype(jnp.float32)
    angles = jnp.stack([grid_row[:, None] * inverse, grid_col[:, None] * inverse], axis=1)
    cosine = jnp.cos(angles)[:, None, None]
    sine = jnp.sin(angles)[:, None, None]
    parts = normed.reshape(normed.shape[:-1] + (2, 2, quarter))
    first = parts[..., 0, :]
    second = parts[..., 1, :]
    turned = jnp.stack([first * cosine - second * sine, second * cosine + first * sine], axis=-2)
    return turned.reshape(normed.shape)


def prepare(data, positions, gain):
    heads = data.astype(jnp.float32).reshape(data.shape[0], data.shape[1], -1, HEAD_DIM)
    normed = heads * lax.rsqrt(jnp.mean(heads * heads, axis=-1, keepdims=True) + EPS) * gain
    return turn(normed, positions).astype(jnp.bfloat16)


def per_device(
    queries,
    keys,
    values,
    query_gain,
    key_gain,
    out_weight,
    moe_tokens,
    moe_gain,
    routes,
    route_weight,
    w_gate,
    w_up,
    w_down,
):
    pos_count = queries.shape[0]
    seq_count = queries.shape[1]
    positions = lax.axis_index("ep") * pos_count + jnp.arange(pos_count, dtype=jnp.int32)
    q_rot = prepare(queries, positions, query_gain)
    k_rot = prepare(keys, positions, key_gain)
    kv_local = k_rot.shape[2]
    groups = q_rot.shape[2] // kv_local
    value_heads = values.reshape(pos_count, seq_count, kv_local, HEAD_DIM)
    q_group = q_rot.reshape(pos_count, seq_count, kv_local, groups, HEAD_DIM)
    scale = HEAD_DIM ** (-0.5)
    start_state = (
        jnp.full((seq_count, kv_local, groups, pos_count), -1e30, jnp.float32),
        jnp.zeros((seq_count, kv_local, groups, pos_count), jnp.float32),
        jnp.zeros((pos_count, seq_count, kv_local, groups, HEAD_DIM), jnp.float32),
    )
    carry = start_state
    key_piece, value_piece = in_one_piece((k_rot, value_heads), "ep", 0, 1)
    count = key_piece.shape[0]
    width = math.gcd(count, 512)
    key_split = key_piece.reshape(count // width, width, seq_count, kv_local, HEAD_DIM)
    value_split = value_piece.reshape(count // width, width, seq_count, kv_local, HEAD_DIM)

    def step(state, block):
        best, total, accum = state
        key_block, value_block = block
        scores = (
            jnp.einsum("pskgd,lskd->skgpl", q_group, key_block, preferred_element_type=jnp.float32)
            * scale
        )
        new_best = jnp.maximum(best, jnp.max(scores, axis=-1))
        factor = jnp.exp(best - new_best)
        expo = jnp.exp(scores - new_best[..., None])
        total = total * factor + jnp.sum(expo, axis=-1)
        added = jnp.einsum(
            "skgpl,lskd->pskgd",
            expo.astype(jnp.bfloat16),
            value_block,
            preferred_element_type=jnp.float32,
        )
        accum = accum * jnp.transpose(factor, (3, 0, 1, 2))[..., None] + added
        return ((new_best, total, accum), None)

    carry, _ = lax.scan(step, carry, (key_split, value_split))
    best, total, accum = carry
    mixed = (accum / jnp.transpose(total, (3, 0, 1, 2))[..., None]).astype(jnp.bfloat16)
    mixed = mixed.reshape(pos_count, seq_count, -1)
    rows = mixed
    product = jnp.dot(
        rows.reshape(pos_count // lax.axis_size("tp") * lax.axis_size("tp") * seq_count, -1),
        out_weight,
        preferred_element_type=jnp.float32,
    )
    attended = sum_at_owner(
        product.reshape(
            pos_count // lax.axis_size("tp") * lax.axis_size("tp"), seq_count, -1
        ).astype(jnp.bfloat16),
        "tp",
        0,
    ).astype(jnp.bfloat16)
    tok_count = moe_tokens.shape[0]
    top_count = routes.shape[1]
    experts = lax.axis_size("ep")
    capacity = max(2, (3 * tok_count * top_count + 2 * experts - 1) // (2 * experts))
    token_float = moe_tokens.astype(jnp.float32)
    normed = (
        token_float
        * lax.rsqrt(jnp.mean(token_float * token_float, axis=-1, keepdims=True) + EPS)
        * moe_gain
    ).astype(jnp.bfloat16)
    hits = (routes[:, :, None] == jnp.arange(experts, dtype=jnp.int32)[None, None, :]).astype(
        jnp.float32
    )
    pair_count = tok_count * top_count
    flat_hits = hits.reshape(pair_count, experts)
    pair_index = jnp.arange(pair_count, dtype=jnp.int32)
    earlier = (pair_index[:, None] > pair_index[None, :]).astype(jnp.float32)
    before = jnp.dot(earlier, flat_hits, precision=lax.Precision.HIGHEST)
    rank = jnp.sum(before * flat_hits, axis=-1).astype(jnp.int32).reshape(tok_count, top_count)
    slot = routes * capacity + rank
    table = jnp.arange(experts * capacity, dtype=jnp.int32)
    dispatch = jnp.sum(
        (slot[None, :, :] == table[:, None, None]).astype(jnp.float32), axis=2
    ).astype(jnp.bfloat16)
    send = jnp.dot(dispatch, normed, preferred_element_type=jnp.float32).astype(jnp.bfloat16)

    def expert_hidden(rows):
        gate = jnp.dot(rows, w_gate[0], preferred_element_type=jnp.float32)
        up = jnp.dot(rows, w_up[0], preferred_element_type=jnp.float32)
        return (jax.nn.silu(gate) * up).astype(jnp.bfloat16)

    received = lax.all_to_all(send, "ep", split_axis=0, concat_axis=0, tiled=True)

    def hidden_rows(piece, start):
        return expert_hidden(piece)

    hidden = work_in_pieces(received, "tp", 0, hidden_rows, 0)
    rows = hidden
    result = sum_at_owner(
        jnp.dot(rows, w_down[0], preferred_element_type=jnp.float32).astype(jnp.bfloat16), "tp", 0
    ).astype(jnp.bfloat16)
    returned_rows = lax.all_to_all(result, "ep", split_axis=0, concat_axis=0, tiled=True)
    combined = jnp.zeros((tok_count, returned_rows.shape[-1]), jnp.float32)
    for choice_index in range(top_count):
        picker = (slot[:, choice_index : choice_index + 1] == table[None, :]).astype(jnp.bfloat16)
        picked = jnp.dot(picker, returned_rows, preferred_element_type=jnp.float32)
        combined = combined + picked * route_weight[:, choice_index : choice_index + 1]
    return (attended, combined.astype(jnp.bfloat16))


def solution(mesh):
    in_specs = (
        P("ep", None, "tp"),
        P("ep", None, "tp"),
        P("ep", None, "tp"),
        P(),
        P(),
        P("tp", None),
        P(("ep", "tp"), None),
        P(),
        P(("ep", "tp"), None),
        P(("ep", "tp"), None),
        P("ep", None, "tp"),
        P("ep", None, "tp"),
        P("ep", "tp", None),
    )
    out_specs = (P(("ep", "tp"), None, None), P(("ep", "tp"), None))
    return jax.shard_map(
        per_device, mesh=mesh, in_specs=in_specs, out_specs=out_specs, check_vma=False
    )
```

profile of v0, /device:TPU:1, one launch (start us, length us, event | category | flops | bytes accessed | tf_op | source)
XLA Modules:
  0.0 458.8 jit_solution(4920895802015456262)
XLA Ops:
  10.7 2.9 convolution_convert_fusion.2
  13.5 2.5 all_to_all.21
  16.0 62.5 %all_to_all.31 = bf16[64,6,2048]{2,1,0:T(8,128)(2,1)S(1)} all-to-all(bf16[64,6,2048]{2,1,0:T(8,128)(2,1)S(1)} %all_to_all.21), channel_id=1, replica_groups=mesh['ep'=64,'tp'=4] {'ep'}, dimensions={0} | all-to-all | bytes 3145728 | tf_op jit(solution)/shard_map/all_to_all | solution.py:178
  82.3 37.4 %all-gather.6.cloned.1.call-done = bf16[4,192,2048]{2,1,0:T(8,128)(2,1)} async-done(((bf16[1,192,2048]{2,1,0:T(8,128)(2,1)}), bf16[4,192,2048]{2,1,0:T(8,128)(2,1)}) %all-gather.6.cloned.1.call-update) | async-done | bytes 3145744 | tf_op jit(solution)/shard_map/all_gather | solution.py:47
  119.7 2.9 fusion.37
  122.6 41.2 %all-gather.8.cloned.1.call-done = bf16[4,192,2048]{2,1,0:T(8,128)(2,1)} async-done(((bf16[1,192,2048]{2,1,0:T(8,128)(2,1)}), bf16[4,192,2048]{2,1,0:T(8,128)(2,1)}) %all-gather.8.cloned.1.call-update) | async-done | bytes 3145744 | tf_op jit(solution)/shard_map/all_gather | solution.py:47
  163.8 3.0 fusion.35
  169.9 4.4 convolution_convert_fusion
  174.2 5.4 %all-to-all-start.2 = ((bf16[4,384,2048]{2,1,0:T(8,128)(2,1)}), bf16[4,384,2048]{2,1,0:T(8,128)(2,1)}, u32[]{:S(2)}, u32[]{:S(2)}) async-start(bf16[4,384,2048]{2,1,0:T(8,128)(2,1)} %bitcast.142), calls=%async_computation.2 | async-start | bytes 12582912 | tf_op jit(solution)/shard_map/all_to_all | solution.py:33
  180.3 70.0 %all-to-all-done.2 = bf16[4,384,2048]{2,1,0:T(8,128)(2,1)} async-done(((bf16[4,384,2048]{2,1,0:T(8,128)(2,1)}), bf16[4,384,2048]{2,1,0:T(8,128)(2,1)}, u32[]{:S(2)}, u32[]{:S(2)}) %all-to-all-start.2) | async-done | bytes 6291488 | tf_op jit(solution)/shard_map/all_to_all | solution.py:33
  250.2 4.2 reduce_sum.86
  256.1 11.7 %all-to-all-start.3 = ((bf16[64,6,2048]{2,1,0:T(8,128)(2,1)}), bf16[64,6,2048]{2,1,0:T(8,128)(2,1)S(1)}, u32[]{:S(2)}, u32[]{:S(2)}) async-start(bf16[64,6,2048]{2,1,0:T(8,128)(2,1)} %all_to_all.24), calls=%async_computation.3 | async-start | bytes 4194304 | tf_op jit(solution)/shard_map/all_to_all | solution.py:188
  267.8 3.9 fusion.54
  271.7 2.6 copy.77
  274.3 2.6 copy.78
  276.9 138.0 %while.15 = (s32[]{:T(128)}, f32[2,1,4,256]{3,2,0,1:T(4,128)S(1)}, f32[2,1,4,256]{3,2,0,1:T(4,128)S(1)}, f32[256,2,1,4,64]{0,4,3,1,2:T(8,128)S(1)}, bf16[32,512,...) while((s32[]{:T(128)}, f32[2,1,4,256]{3,2,0,1:T(4,128)S(1)}, ...), condition=%wide.region_5.6_spmd.clone, body=%wide.region_2.5_spmd.clone.sunk | while | flops 277229568 | bytes 14286969 | solution.py:130
  279.3 1.9 fusion.74
  287.9 1.9 fusion.74
  292.2 1.9 fusion.74
  296.5 1.9 fusion.74
  300.8 1.9 fusion.74
  305.1 1.9 fusion.74
  309.4 1.9 fusion.74
  313.8 1.9 fusion.74
  318.1 1.9 fusion.74
  322.4 1.9 fusion.74
  326.7 1.9 fusion.74
  331.0 1.9 fusion.74
  335.3 1.9 fusion.74
  339.6 1.9 fusion.74
  343.9 1.9 fusion.74
  348.2 1.9 fusion.74
  352.6 1.9 fusion.74
  369.8 1.9 fusion.74
  374.1 1.9 fusion.74
  378.4 1.9 fusion.74
  382.7 1.9 fusion.74
  387.1 1.9 fusion.74
  391.4 1.9 fusion.74
  395.7 1.9 fusion.74
  400.0 1.9 fusion.74
  404.3 1.9 fusion.74
  408.6 1.9 fusion.74
  414.9 2.0 convolution_convert_fusion.1
  418.3 4.6 all-to-all-start
  423.0 2.6 all_to_all.26
  427.4 21.6 %all-to-all-done = bf16[4,64,2,2048]{3,1,2,0:T(8,128)(2,1)} async-done(((bf16[4,64,2,2048]{3,1,2,0:T(8,128)(2,1)}), bf16[4,64,2,2048]{3,1,2,0:T(8,128)(2,1)}, u32[]{:S(2)}, u32[]{:S(2)}) %all-to-all-start) | async-done | bytes 2097184 | tf_op jit(solution)/shard_map/all_to_all | solution.py:33
  448.9 2.0 reduce_sum.82
  (243 shorter events, 103.3 us)
Async XLA Ops:
  7.2 162.7 %copy-start = (bf16[1,256,2048]{2,1,0:T(8,128)(2,1)S(1)}, bf16[1,256,2048]{2,1,0:T(8,128)(2,1)}, u32[]{:S(2)}) copy-start(bf16[1,256,2048]{2,1,0:T(8,128)(2,1)} %param.27) | copy-start | bytes 3145732
  7.2 112.5 %all-gather.6.cloned.1.call-start = ((), (), s32[]{:S(2)}) async-start(), calls=%async_computation.5 | async-start | bytes 3932160 | tf_op jit(solution)/shard_map/all_gather | solution.py:47
  78.6 2.8 copy-start.3
  78.7 2.8 copy-start.7
  78.7 2.9 copy-start.5
  79.8 39.9 %copy-start.11 = (bf16[1,2048,256]{2,1,0:T(8,128)(2,1)S(1)}, bf16[1,2048,256]{2,1,0:T(8,128)(2,1)}, u32[]{:S(2)}) copy-start(bf16[1,2048,256]{2,1,0:T(8,128)(2,1)} %param.25) | copy-start | bytes 3145732
  79.9 83.9 %all-gather.8.cloned.1.call-start = ((), (), s32[]{:S(2)}) async-start(), calls=%async_computation.6 | async-start | bytes 3932160 | tf_op jit(solution)/shard_map/all_gather | solution.py:47
  81.1 186.7 %all-gather.4.cloned.1.call-start = ((), (), s32[]{:S(2)}) async-start(), calls=%async_computation.4 | async-start | bytes 8519680 | tf_op jit(solution)/shard_map/all_gather | solution.py:22
  163.8 3.0 copy-start.9
  163.8 3.1 copy-start.12
  166.9 1.9 copy-start.10
  174.2 5.5 %copy-start.8 = (f32[64]{0:T(128)S(1)}, f32[64]{0:T(128)}, u32[]{:S(2)}) copy-start(f32[64]{0:T(128)} %param.18) | copy-start | bytes 772
  174.2 5.5 %copy-start.4 = (bf16[256,2,256]{2,1,0:T(2,128)(2,1)S(1)}, bf16[256,2,256]{2,1,0:T(2,128)(2,1)}, u32[]{:S(2)}) copy-start(bf16[256,2,256]{2,1,0:T(2,128)(2,1)} %param.15) | copy-start | bytes 786436
  174.2 76.0 %all-to-all-start.2 = ((bf16[4,384,2048]{2,1,0:T(8,128)(2,1)}), bf16[4,384,2048]{2,1,0:T(8,128)(2,1)}, u32[]{:S(2)}, u32[]{:S(2)}) async-start(bf16[4,384,2048]{2,1,0:T(8,128)(2,1)} %bitcast.142), calls=%async_computation.2 | async-start | bytes 12582912 | tf_op jit(solution)/shard_map/all_to_all | solution.py:33
  256.1 162.2 %all-to-all-start.3 = ((bf16[64,6,2048]{2,1,0:T(8,128)(2,1)}), bf16[64,6,2048]{2,1,0:T(8,128)(2,1)S(1)}, u32[]{:S(2)}, u32[]{:S(2)}) async-start(bf16[64,6,2048]{2,1,0:T(8,128)(2,1)} %all_to_all.24), calls=%async_computation.3 | async-start | bytes 4194304 | tf_op jit(solution)/shard_map/all_to_all | solution.py:188
  418.3 4.6 %copy-start.6 = (f32[128,2]{0,1:T(2,128)S(1)}, f32[128,2]{0,1:T(2,128)}, u32[]{:S(2)}) copy-start(f32[128,2]{0,1:T(2,128)} %param.24) | copy-start | bytes 3076
  418.3 4.6 %copy-start.2 = (bf16[64,6,2048]{2,1,0:T(8,128)(2,1)}, bf16[64,6,2048]{2,1,0:T(8,128)(2,1)S(1)}, u32[]{:S(2)}) copy-start(bf16[64,6,2048]{2,1,0:T(8,128)(2,1)S(1)} %all-to-all-done.3) | copy-start | bytes 4718596
  418.3 30.6 %all-to-all-start = ((bf16[4,64,2,2048]{3,1,2,0:T(8,128)(2,1)}), bf16[4,64,2,2048]{3,1,2,0:T(8,128)(2,1)}, u32[]{:S(2)}, u32[]{:S(2)}) async-start(bf16[4,64,2,2048]{3,1,2,0:T(8,128)(2,1)} %copy.63), calls=%async_computation | async-start | bytes 4194304 | tf_op jit(solution)/shard_map/all_to_all | solution.py:33
  426.1 26.2 %copy-start.1 = (bf16[1,256,2048]{2,1,0:T(8,128)(2,1)S(1)}, bf16[1,256,2048]{2,1,0:T(8,128)(2,1)}, u32[]{:S(2)}) copy-start(bf16[1,256,2048]{2,1,0:T(8,128)(2,1)} %param.27) | copy-start | bytes 3145732
Sparse Core Ops, SparseCore 0:
  80.0 39.6 all-gather.5
  121.5 42.2 all-gather.7
  167.0 85.7 all-gather.3
where the time goes:
time: 461 us; the launch traced here: 459 us
  waiting for transfers between devices  170 us (37%)
  matrix products  132 us (29%)
  blocking collectives  62.5 us (14%)
  other arithmetic  33.4 us (7%)
  local copies, waits for them, and re-layouts  23.5 us (5%)
  starting transfers between devices  21.8 us (5%)
  between operations  14.1 us (3%)
    all_to_all x2, waiting for transfers between devices, sum_at_owner(): lax.all_to_all(tiles, axis, split_axis=0, concat_axis=0, tiled=True)  91.5 us
    all_gather x2, waiting for transfers between devices, work_in_pieces(): tiles = [lax.all_gather(piece, axis) for piece in pieces]  78.6 us
    all_to_all x1, blocking collectives, per_device(): lax.all_to_all(send, 'ep', split_axis=0, concat_axis=0, tiled=True)  62.5 us
    dot_general x32, matrix products, step(): jnp.einsum('skgpl,lskd->pskgd', expo.astype(jnp.bfloat16), value_block, p...  59.4 us
    dot_general x32, matrix products, step(): jnp.einsum('pskgd,lskd->skgpl', q_group, key_block, preferred_element_typ...  53.3 us
    reduce_sum x32, other arithmetic, step(): total = total * factor + jnp.sum(expo, axis=-1)  22.6 us
    all_to_all x1, starting transfers between devices, per_device(): lax.all_to_all(result, 'ep', split_axis=0, concat_axis=0, tiled=True)  11.7 us
    all_to_all x2, starting transfers between devices, sum_at_owner(): lax.all_to_all(tiles, axis, split_axis=0, concat_axis=0, tiled=True)  10 us
  transfers between devices with their start and end apart: 6, of which 4 were waited for; matrix products, arithmetic and copies ran while one was open for 37% of the time, Pallas kernels for 0%

commit v1 on v0

v1 whole, which is shorter than its diff:
```python
import functools

import jax
import jax.numpy as jnp
from jax import lax
from jax.experimental import pallas as pl
from jax.experimental.pallas import tpu as pltpu
from jax.sharding import PartitionSpec as P

HEAD_DIM = 64
GRID_W = 64
EPS = 1e-06
THETA = 10000.0
CAP = 6
SLOT = 8
PACK = 1536
TAIL = 512
PLANE = 8
PLANES = 8
BLOCK = 256
QW = 1024
CHUNK = 2
LOG2E = 1.4426950408889634
MESH = pl.DeviceIdType.MESH
BF16 = jnp.bfloat16
F32 = jnp.float32


def rcopy(src, dst, send_sem, recv_sem, dev):
    return pltpu.make_async_remote_copy(
        src_ref=src,
        dst_ref=dst,
        send_sem=send_sem,
        recv_sem=recv_sem,
        device_id=dev,
        device_id_type=MESH,
    )


def wait_for(ref, sem):
    pltpu.make_async_copy(ref, ref, sem).wait()


def near_first(i):
    return (1 - 2 * lax.rem(i + 1, 2)) * ((i + 1) // 2)


def attend(group, tile, q2, kvbuf, s_ref, m_ref, acc_ref):
    scale = LOG2E * HEAD_DIM**-0.5
    cols = pl.ds(pl.multiple_of(tile * QW, QW), QW)
    pieces = PLANE // CHUNK
    m_old = m_ref[tile]
    for h in range(2):
        q = q2[h, :, cols]
        for p in range(pieces):
            k = kvbuf[pl.ds(group * PLANE + p * CHUNK, CHUNK), 0:128, :].reshape(CHUNK * 128, 128)
            s_ref[h, p] = jnp.dot(k, q, preferred_element_type=F32)
    best = m_old
    for h in range(2):
        for p in range(pieces):
            part = s_ref[h, p].reshape(CHUNK * 16, 8, QW)
            best = jnp.maximum(best, jnp.max(part, axis=0))
    top = jnp.max(best, axis=0, keepdims=True)
    m_new = jnp.broadcast_to(top, (8, QW))
    factor = jnp.exp2((m_old - m_new) * scale)
    shift = top * scale
    m_ref[tile] = m_new
    acc = acc_ref[tile] * jnp.broadcast_to(factor[0:1], (acc_ref.shape[1], QW))
    ones = jnp.ones((16, CHUNK * 128), BF16)
    for h in range(2):
        for p in range(pieces):
            probs = jnp.exp2(s_ref[h, p] * scale - shift).astype(BF16)
            v = jnp.concatenate(
                [
                    kvbuf[group * PLANE + p * CHUNK + b, 128 + 64 * h : 192 + 64 * h, :]
                    for b in range(CHUNK)
                ],
                axis=1,
            )
            acc = acc + jnp.dot(
                jnp.concatenate([v, ones], axis=0), probs, preferred_element_type=F32
            )
    acc_ref[tile] = acc


def kernel(
    send,
    kvp,
    qt,
    wg,
    wu,
    wd,
    wo,
    unpack,
    pack,
    ret,
    out_parts,
    recv,
    recv2,
    xbuf,
    wgb,
    wub,
    wdb,
    ybuf,
    part,
    rs,
    ret_send,
    kvbuf,
    qbuf,
    q2,
    s_ref,
    m_ref,
    acc_ref,
    obuf,
    sem_local,
    sem_send,
    sem_w,
    sem_d,
    sem_f,
    sem_rs,
    sem_ret,
    sem_x,
    sem_up,
    sem_down,
    sem_q,
    sem_o,
):
    me = lax.axis_index("ep")
    y = lax.axis_index("tp")
    z = me // PLANE
    inner = lax.rem(me, PLANE)
    core = lax.rem(me, 2)
    base = z * PLANE
    y_w = y + 1 - 2 * lax.rem(y, 2)
    y_t = 3 - y
    tiles = qbuf.shape[0] * qbuf.shape[2] // QW

    other = me + 1 - 2 * core
    q_copy = rcopy(qt.at[1 - core], qbuf.at[core], sem_send.at[0], sem_q, (other, y))
    q_copy.start()
    q_local = pltpu.make_async_copy(qt.at[core], qbuf.at[core], sem_local.at[0])

    def plane_peer(j):
        return lax.rem(inner + j, PLANE)

    def x_send(j, _):
        peer = plane_peer(j)
        rcopy(
            kvp.at[lax.rem(peer, 2)],
            kvbuf.at[me],
            sem_send.at[1],
            sem_x.at[inner],
            (base + peer, y),
        ).start()
        return 0

    lax.fori_loop(1, PLANE, x_send, 0)
    kv_local = pltpu.make_async_copy(kvp.at[core], kvbuf.at[me], sem_local.at[1])
    kv_local.start()

    w_copies = []
    for i, (src, dst) in enumerate(((wg, wgb), (wu, wub), (wd, wdb))):
        w_copy = rcopy(src, dst.at[1], sem_send.at[2 + i], sem_w.at[i], (me, y_w))
        w_copy.start()
        w_copies.append(w_copy)
    w_local = []
    for i, (src, dst) in enumerate(((wg, wgb), (wu, wub), (wd, wdb))):
        local = pltpu.make_async_copy(src, dst.at[0], sem_local.at[2 + i])
        local.start()
        w_local.append(local)

    def plane_at(i, sign):
        return lax.rem(z + sign * near_first(i) + 2 * PLANES, PLANES)

    def d_send(t, _):
        to = plane_at(t // PLANE, 1) * PLANE + lax.rem(t + inner, PLANE)

        @pl.when(to != me)
        def _():
            rcopy(send.at[to], recv.at[me], sem_send.at[5], sem_d.at[me], (to, y)).start()

        return 0

    lax.fori_loop(0, PLANES * PLANE, d_send, 0)
    d_local = pltpu.make_async_copy(send.at[me], recv.at[me], sem_local.at[5])
    d_local.start()

    q_local.start()
    m_ref[...] = jnp.full(m_ref.shape, -1e30, F32)
    acc_ref[...] = jnp.zeros(acc_ref.shape, F32)

    kv_local.wait()

    def x_wait(j, _):
        peer = plane_peer(j)
        wait_for(kvbuf.at[base + peer], sem_x.at[peer])
        return 0

    lax.fori_loop(1, PLANE, x_wait, 0)
    up = lax.rem(z + 1, PLANES) * PLANE + inner
    down = lax.rem(z + PLANES - 1, PLANES) * PLANE + inner

    def group_of(shift):
        return lax.rem(z + shift + 2 * PLANES, PLANES)

    def group_ref(group):
        return kvbuf.at[pl.ds(pl.multiple_of(group * PLANE, PLANE), PLANE)]

    def ring_up(step):
        g = group_ref(group_of(1 - step))
        rcopy(g, g, sem_send.at[6], sem_up.at[step - 1], (up, y)).start()

    def ring_down(step):
        g = group_ref(group_of(step - 1))
        rcopy(g, g, sem_send.at[7], sem_down.at[step - 1], (down, y)).start()

    def ring_wait_up(step):
        wait_for(group_ref(group_of(-step)), sem_up.at[step - 1])

    def ring_wait_down(step):
        wait_for(group_ref(group_of(step)), sem_down.at[step - 1])

    ring_up(1)
    ring_down(1)

    q_local.wait()
    q_copy.wait_recv()
    zeros = jnp.zeros((64, qbuf.shape[2]), BF16)
    for s in range(2):
        cols = slice(s * qbuf.shape[2], (s + 1) * qbuf.shape[2])
        q2[0, 0:64, cols] = qbuf[s]
        q2[0, 64:128, cols] = zeros
        q2[1, 0:64, cols] = zeros
        q2[1, 64:128, cols] = qbuf[s]

    def attend_groups(first, last):
        def body(i, _):
            n = first + i // tiles
            group = lax.rem(z - near_first(n) + 2 * PLANES, PLANES)
            attend(group, lax.rem(i, tiles), q2, kvbuf, s_ref, m_ref, acc_ref)
            return 0

        lax.fori_loop(0, (last - first) * tiles, body, 0)

    attend_groups(0, 1)

    def open_rows(src, plane, row0):
        rows = src[pl.ds(pl.multiple_of(plane * PLANE, PLANE), PLANE)].reshape(PLANE * SLOT, PACK)
        at = pl.ds(pl.multiple_of(row0 + plane * PLANE * CAP, 16), PLANE * CAP)
        main = jnp.dot(unpack[0], rows, preferred_element_type=F32)
        xbuf[at, 0:PACK] = main.astype(BF16)
        tail = jnp.dot(unpack[1], rows[:, 0:TAIL], preferred_element_type=F32)
        for k in range(1, 3):
            tail = tail + jnp.dot(
                unpack[1 + k], rows[:, k * TAIL : (k + 1) * TAIL], preferred_element_type=F32
            )
        xbuf[at, PACK : PACK + TAIL] = tail.astype(BF16)

    d_local.wait()

    def plane_ref(ref, plane):
        return ref.at[pl.ds(pl.multiple_of(plane * PLANE, PLANE), PLANE)]

    def arrive(i, _):
        plane = plane_at(i, -1)

        def one(j, _):
            src = plane * PLANE + j

            @pl.when(src != me)
            def _():
                wait_for(recv.at[src], sem_d.at[src])

            return 0

        lax.fori_loop(0, PLANE, one, 0)
        rcopy(
            plane_ref(recv, plane),
            plane_ref(recv2, plane),
            sem_send.at[8],
            sem_f.at[plane],
            (me, y_t),
        ).start()
        open_rows(recv, plane, 0)
        return 0

    lax.fori_loop(0, PLANES, arrive, 0)

    rows_own = PLANES * PLANE * CAP

    def arrive2(i, _):
        plane = lax.rem(z - near_first(i) + 2 * PLANES, PLANES)
        wait_for(plane_ref(recv2, plane), sem_f.at[plane])
        open_rows(recv2, plane, rows_own)
        return 0

    lax.fori_loop(0, PLANES, arrive2, 0)

    def ffn(blk, n):
        at = pl.ds(pl.multiple_of(n * 192, 16), 192)
        x = xbuf[at]
        gate = jnp.dot(x, wgb[blk], preferred_element_type=F32)
        lift = jnp.dot(x, wub[blk], preferred_element_type=F32)
        hidden = (jax.nn.silu(gate) * lift).astype(BF16)
        ybuf[blk, at, :] = jnp.dot(hidden, wdb[blk], preferred_element_type=F32).astype(BF16)

    for local in w_local:
        local.wait()

    def ffn_own(n, _):
        ffn(0, n)
        return 0

    lax.fori_loop(0, 4, ffn_own, 0)

    ring_wait_up(1)
    ring_wait_down(1)
    ring_up(2)
    ring_down(2)

    for w_copy in w_copies:
        w_copy.wait_recv()

    def share(n, _):
        ffn(1, 2 + n)

        def piece(j, _):
            plane = n * 4 + j
            at = pl.ds(pl.multiple_of(rows_own + plane * 48, 16), 48)
            both = ybuf[0, at, :].astype(F32) + ybuf[1, at, :].astype(F32)
            part[plane] = both.astype(BF16)
            return 0

        lax.fori_loop(0, 4, piece, 0)
        four = pl.ds(pl.multiple_of(n * 4, 4), 4)
        rcopy(part.at[four], rs.at[four], sem_send.at[9], sem_rs.at[n], (me, y_t)).start()
        return 0

    lax.fori_loop(0, 2, share, 0)

    def ffn_rest(n, _):
        ffn(1, n)
        return 0

    lax.fori_loop(0, 2, ffn_rest, 0)

    attend_groups(1, 3)
    ring_wait_up(2)
    ring_wait_down(2)
    ring_up(3)
    ring_down(3)

    def give_back(n, _):
        four = pl.ds(pl.multiple_of(n * 4, 4), 4)
        wait_for(rs.at[four], sem_rs.at[n])

        def one(i, _):
            plane = n * 4 + i
            at = pl.ds(pl.multiple_of(plane * 48, 16), 48)
            total = (
                ybuf[0, at, :].astype(F32) + ybuf[1, at, :].astype(F32) + rs[plane].astype(F32)
            ).astype(BF16)
            last = total[:, PACK : PACK + TAIL]
            for k in range(3):
                packed = jnp.dot(
                    pack[0], total[:, k * TAIL : (k + 1) * TAIL], preferred_element_type=F32
                ) + jnp.dot(pack[1 + k], last, preferred_element_type=F32)
                ret_send[
                    pl.ds(pl.multiple_of(plane * PLANE, PLANE), PLANE),
                    :,
                    k * TAIL : (k + 1) * TAIL,
                ] = packed.astype(BF16).reshape(PLANE, SLOT, TAIL)
            return 0

        lax.fori_loop(0, 4, one, 0)

        def out(j, _):
            to = n * 32 + lax.rem(j + inner, 32)

            @pl.when(to != me)
            def _():
                rcopy(
                    ret_send.at[to], ret.at[me], sem_send.at[10], sem_ret.at[me], (to, y)
                ).start()

            @pl.when(to == me)
            def _():
                pltpu.make_async_copy(ret_send.at[to], ret.at[me], sem_local.at[6]).start()

            return 0

        lax.fori_loop(0, 32, out, 0)
        return 0

    lax.fori_loop(0, 2, give_back, 0)

    attend_groups(3, 5)
    ring_wait_up(3)
    ring_wait_down(3)
    ring_up(4)
    attend_groups(5, 7)
    ring_wait_up(4)
    attend_groups(7, 8)

    def project(s, _):
        acc = acc_ref[s]
        mixed = (acc[0:64] / acc[64:65]).astype(BF16).astype(F32)
        heads = jnp.concatenate(
            [mixed[:, h * BLOCK : (h + 1) * BLOCK].T for h in range(QW // BLOCK)], axis=1
        ).astype(BF16)
        obuf[s] = jnp.dot(heads, wo[...], preferred_element_type=F32).astype(BF16)
        return 0

    lax.fori_loop(0, 2, project, 0)

    def o_send(j, _):
        to_y = lax.rem(y + j // 2, 4)
        to_core = lax.rem(core + j, 2)
        src = obuf.at[to_core, pl.ds(pl.multiple_of(to_y * 64, 64), 64)]
        rcopy(
            src,
            out_parts.at[core, y],
            sem_send.at[11],
            sem_o.at[core * 4 + y],
            (me - core + to_core, to_y),
        ).start()
        return 0

    lax.fori_loop(1, 8, o_send, 0)
    o_local = pltpu.make_async_copy(
        obuf.at[core, pl.ds(pl.multiple_of(y * 64, 64), 64)], out_parts.at[core, y], sem_local.at[7]
    )
    o_local.start()

    def o_wait(j, _):
        from_y = lax.rem(y + j // 2, 4)
        from_core = lax.rem(core + j, 2)
        wait_for(out_parts.at[from_core, from_y], sem_o.at[from_core * 4 + from_y])
        return 0

    lax.fori_loop(1, 8, o_wait, 0)
    o_local.wait()

    def ret_wait(j, _):
        src = lax.rem(me + j, 64)
        wait_for(ret.at[src], sem_ret.at[src])
        return 0

    lax.fori_loop(1, 64, ret_wait, 0)
    wait_for(ret.at[me], sem_local.at[6])

    q_copy.wait_send()
    wait_for(kvbuf.at[pl.ds(0, 7)], sem_send.at[1])
    for w_copy in w_copies:
        w_copy.wait_send()
    wait_for(recv.at[pl.ds(0, 63)], sem_send.at[5])
    wait_for(kvbuf.at[pl.ds(0, 32)], sem_send.at[6])
    wait_for(kvbuf.at[pl.ds(0, 24)], sem_send.at[7])
    wait_for(recv, sem_send.at[8])
    wait_for(part, sem_send.at[9])
    wait_for(recv.at[pl.ds(0, 63)], sem_send.at[10])
    wait_for(xbuf.at[pl.ds(0, 448)], sem_send.at[11])


def call_kernel(send, kvp, qt, wg, wu, wd, wo, unpack, pack):
    any_space = pl.BlockSpec(memory_space=pl.ANY)
    vmem = pl.BlockSpec(memory_space=pltpu.VMEM)
    dma = pltpu.SemaphoreType.DMA
    n_tiles = 2 * qt.shape[2] // QW
    return pl.pallas_call(
        kernel,
        out_shape=(
            jax.ShapeDtypeStruct(send.shape, BF16),
            jax.ShapeDtypeStruct((2, 4, 64, wo.shape[1]), BF16),
        ),
        in_specs=[any_space] * 6 + [vmem] * 3,
        out_specs=(any_space, any_space),
        scratch_shapes=[
            pltpu.VMEM(send.shape, BF16),
            pltpu.VMEM(send.shape, BF16),
            pltpu.VMEM((768, 2048), BF16),
            pltpu.VMEM((2,) + wg.shape, BF16),
            pltpu.VMEM((2,) + wu.shape, BF16),
            pltpu.VMEM((2,) + wd.shape, BF16),
            pltpu.VMEM((2, 768, 2048), BF16),
            pltpu.VMEM((8, 48, 2048), BF16),
            pltpu.VMEM((8, 48, 2048), BF16),
            pltpu.VMEM(send.shape, BF16),
            pltpu.VMEM((64, 256, 128), BF16),
            pltpu.VMEM((2,) + qt.shape[1:], BF16),
            pltpu.VMEM((2, 128, 2 * qt.shape[2]), BF16),
            pltpu.VMEM((2, PLANE // CHUNK, CHUNK * 128, QW), F32),
            pltpu.VMEM((n_tiles, 8, QW), F32),
            pltpu.VMEM((n_tiles, 80, QW), F32),
            pltpu.VMEM((2, BLOCK, wo.shape[1]), BF16),
            dma((8,)),
            dma((12,)),
            dma((3,)),
            dma((64,)),
            dma((8,)),
            dma((2,)),
            dma((64,)),
            dma((8,)),
            dma((4,)),
            dma((3,)),
            dma(()),
            dma((8,)),
        ],
        compiler_params=pltpu.CompilerParams(has_side_effects=True, vmem_limit_bytes=60 * 2**20),
        name="mega",
    )(send, kvp, qt, wg, wu, wd, wo, unpack, pack)


def turn(normed, positions):
    quarter = normed.shape[-1] // 4
    inverse = THETA ** (-jnp.arange(quarter, dtype=F32) / quarter)
    grid_row = (positions // GRID_W).astype(F32)
    grid_col = (positions % GRID_W).astype(F32)
    angles = jnp.stack([grid_row[:, None] * inverse, grid_col[:, None] * inverse], axis=1)
    cosine = jnp.cos(angles)[:, None, None]
    sine = jnp.sin(angles)[:, None, None]
    parts = normed.reshape(normed.shape[:-1] + (2, 2, quarter))
    first = parts[..., 0, :]
    second = parts[..., 1, :]
    turned = jnp.stack([first * cosine - second * sine, second * cosine + first * sine], axis=-2)
    return turned.reshape(normed.shape)


def prepare(data, positions, gain):
    heads = data.astype(F32).reshape(data.shape[0], data.shape[1], -1, HEAD_DIM)
    normed = heads * lax.rsqrt(jnp.mean(heads * heads, axis=-1, keepdims=True) + EPS) * gain
    return turn(normed, positions).astype(BF16)


def one_hot_packing():
    row = jnp.arange(PLANE * CAP, dtype=jnp.int32)[:, None]
    col = jnp.arange(PLANE * SLOT, dtype=jnp.int32)[None, :]
    same = row // CAP == col // SLOT
    r, s = row % CAP, col % SLOT
    picks = [same & (r == s)] + [same & (s == CAP + r // 3) & (r % 3 == k) for k in range(3)]
    unpack = jnp.stack(picks).astype(BF16)
    return unpack, jnp.swapaxes(unpack, 1, 2)


def per_device(
    queries,
    keys,
    values,
    query_gain,
    key_gain,
    out_weight,
    moe_tokens,
    moe_gain,
    routes,
    route_weight,
    w_gate,
    w_up,
    w_down,
):
    pos_count, seq_count = queries.shape[0], queries.shape[1]
    positions = lax.axis_index("ep") * pos_count + jnp.arange(pos_count, dtype=jnp.int32)
    q_rot = prepare(queries, positions, query_gain)
    k_rot = prepare(keys, positions, key_gain)[:, :, 0]
    qt = jnp.transpose(q_rot, (1, 3, 2, 0)).reshape(seq_count, HEAD_DIM, -1)
    half = pos_count // 2
    k_two = jnp.concatenate([k_rot[:half], k_rot[half:]], axis=-1)
    k_two = jnp.transpose(k_two, (1, 0, 2))
    v_two = jnp.transpose(values.reshape(2, half, seq_count, HEAD_DIM), (2, 0, 3, 1))
    kvp = jnp.concatenate([k_two, v_two.reshape(seq_count, 2 * HEAD_DIM, half)], axis=1)

    tok_count, top_count = routes.shape
    experts = lax.axis_size("ep")
    token_float = moe_tokens.astype(F32)
    normed = (
        token_float
        * lax.rsqrt(jnp.mean(token_float * token_float, axis=-1, keepdims=True) + EPS)
        * moe_gain
    ).astype(BF16)
    hits = (routes[:, :, None] == jnp.arange(experts, dtype=jnp.int32)[None, None, :]).astype(BF16)
    pair_count = tok_count * top_count
    flat_hits = hits.reshape(pair_count, experts)
    pair_index = jnp.arange(pair_count, dtype=jnp.int32)
    earlier = (pair_index[:, None] > pair_index[None, :]).astype(BF16)
    before = jnp.dot(earlier, flat_hits, preferred_element_type=F32)
    rank = jnp.sum(before * flat_hits.astype(F32), axis=-1).astype(jnp.int32)
    rank = rank.reshape(tok_count, top_count)
    main = routes * SLOT + rank
    rest = routes * SLOT + CAP + rank // 3
    third = rank % 3
    table = jnp.arange(experts * SLOT, dtype=jnp.int32)

    def spread(slot, keep):
        hit = (slot[None, :, :] == table[:, None, None]) & keep[None]
        return jnp.any(hit, axis=2).astype(BF16)

    first = spread(main, third >= 0)
    columns = []
    for k in range(3):
        lhs = jnp.concatenate([first, spread(rest, third == k)], axis=1)
        rhs = jnp.concatenate(
            [normed[:, k * TAIL : (k + 1) * TAIL], normed[:, PACK : PACK + TAIL]], axis=0
        )
        columns.append(jnp.dot(lhs, rhs, preferred_element_type=F32).astype(BF16))
    send = jnp.concatenate(columns, axis=1).reshape(experts, SLOT, PACK)

    unpack, pack = one_hot_packing()
    ret, out_parts = call_kernel(
        send, kvp, qt, w_gate[0], w_up[0], w_down[0], out_weight, unpack, pack
    )

    attended = jnp.transpose(out_parts.astype(F32).sum(axis=1), (1, 0, 2)).astype(BF16)

    rows = ret.reshape(experts * SLOT, PACK)
    combined = jnp.zeros((tok_count, PACK + TAIL), F32)
    for choice in range(top_count):
        pick = slice(choice, choice + 1)
        lead = (main[:, pick] == table[None, :]).astype(BF16)
        picked = jnp.dot(lead, rows, preferred_element_type=F32)
        tail = jnp.zeros((tok_count, TAIL), F32)
        for k in range(3):
            follow = ((rest[:, pick] == table[None, :]) & (third[:, pick] == k)).astype(BF16)
            tail = tail + jnp.dot(
                follow, rows[:, k * TAIL : (k + 1) * TAIL], preferred_element_type=F32
            )
        picked = jnp.concatenate([picked, tail], axis=1)
        combined = combined + picked * route_weight[:, pick]
    return (attended, combined.astype(BF16))


def solution(mesh):
    in_specs = (
        P("ep", None, "tp"),
        P("ep", None, "tp"),
        P("ep", None, "tp"),
        P(),
        P(),
        P("tp", None),
        P(("ep", "tp"), None),
        P(),
        P(("ep", "tp"), None),
        P(("ep", "tp"), None),
        P("ep", None, "tp"),
        P("ep", None, "tp"),
        P("ep", "tp", None),
    )
    out_specs = (P(("ep", "tp"), None, None), P(("ep", "tp"), None))
    return jax.shard_map(
        per_device, mesh=mesh, in_specs=in_specs, out_specs=out_specs, check_vma=False
    )
```

time: 461 us -> 219 us (0.48)
  the two profiles are of different devices: /device:TPU:1 before, /device:TPU:131 now
where the time goes in v1:
time: 219 us; the launch traced here: 218 us
  Pallas kernels  199 us (91%)
  other arithmetic  8.46 us (4%)
  local copies, waits for them, and re-layouts  5.74 us (3%)
  matrix products  3.76 us (2%)
    pallas_call x1, Pallas kernels, call_kernel(): pl.pallas_call(kernel, out_shape=(jax.ShapeDtypeStruct(send.shape, BF16),...  199 us

profile of v1, /device:TPU:131, one launch (start us, length us, event | category | flops | bytes accessed | tf_op | source)
XLA Modules:
  0.0 218.3 jit_solution(7020785391198743210)
XLA Ops:
  0.6 0.0 copy-start
  0.7 1.3 fusion.1
  1.9 1.2 fusion.3
  3.2 0.1 copy.83
  3.3 0.1 eq.353
  3.5 0.2 fusion
  3.7 0.1 convert_element_type.113
  3.9 0.1 copy.84
  4.0 0.3 fusion.11
  4.3 0.3 convolution_convert_fusion
  4.7 0.3 convolution_convert_fusion.1
  5.1 0.3 convolution_convert_fusion.2
  5.5 0.1 pad_maximum_fusion
  5.6 0.0 copy-start.2
  5.6 0.0 copy-start.6
  5.6 1.6 copy.88
  7.2 0.0 copy-done.6
  7.3 0.1 fusion.43
  7.4 0.1 broadcast_multiply_fusion.1
  7.5 0.1 fusion.62
  7.6 0.1 copy.90
  7.8 0.1 copy.89
  7.9 0.1 maximum_bitcast_fusion
  8.0 0.7 pad_maximum_fusion.14.kvp
  8.7 0.1 mul.251
  8.7 0.2 copy.92
  8.9 0.1 bitcast_reduce_fusion
  9.0 0.1 multiply_multiply_fusion
  9.1 0.1 subtract_convert_fusion
  9.3 0.2 copy.100
  9.5 0.9 reshape.806.qt
  10.4 0.1 fusion.65
  10.5 0.6 fusion.76
  11.2 0.7 copy.95.unpack
  11.9 199.4 %mega.1 = (bf16[64,8,1536]{2,1,0:T(8,128)(2,1)}, bf16[2,4,64,2048]{3,2,1,0:T(8,128)(2,1)}) custom-call(bf16[64,8,1536]{2,1,0:T(8,128)(2,1)} %bitcast.63, bf16[2,256,128]{2,1,0:T(8,128)(2,1)} %pad_maximum_fusion.14.kvp, bf16[2,64,1024]{2,1,0:T(8,128)(2,1)} %reshape.806.qt, bf16[2048,256]{1,0:T(8,128)(2,1)} %bitcast.68, bf16[2048,256]{1,0:T(8,128)(2,1)} %bitcast.69, ...), custom_call_target="tpu_custom_call" | custom-call | tf_op jit(solution)/shard_map/mega/pallas_call | solution.py:470
  211.3 0.0 copy-start.1
  211.3 2.1 reduce_sum.52
  213.4 1.3 copy.96
  214.8 0.3 fusion.20
  215.1 0.3 convolution_add_fusion.3
  215.4 0.3 convolution_add_fusion.2
  215.6 0.4 fusion.34
  216.1 0.3 fusion.18
  216.3 0.3 convolution_add_fusion.1
  216.6 0.0 copy-start.5
  216.6 0.3 convolution_add_fusion
  216.9 0.4 fusion.38
  217.4 1.0 fusion.5
  (37 shorter events, 0.5 us)
Async XLA Ops:
  0.6 6.5 %copy-start = (bf16[256,2,64]{0,2,1:T(8,128)(2,1)S(1)}, bf16[256,2,64]{0,2,1:T(8,128)(2,1)}, u32[]{:S(2)}) copy-start(bf16[256,2,64]{0,2,1:T(8,128)(2,1)} %param.15) | copy-start | bytes 196612
  0.6 2.6 %copy-start.4 = (s32[128,2]{0,1:T(2,128)S(1)}, s32[128,2]{0,1:T(2,128)}, u32[]{:S(2)}) copy-start(s32[128,2]{0,1:T(2,128)} %param.21) | copy-start | bytes 3076
  5.6 1.6 copy-start.2
  5.6 1.7 copy-start.6
  7.2 1.5 copy-start.7
  7.2 1.6 copy-start.3
  211.3 3.5 %copy-start.1 = (bf16[64,8,1536]{2,1,0:T(8,128)(2,1)S(1)}, bf16[64,8,1536]{2,1,0:T(8,128)(2,1)}, u32[]{:S(2)}) copy-start(bf16[64,8,1536]{2,1,0:T(8,128)(2,1)} %get-tuple-element.5) | copy-start | bytes 4718596
  216.6 0.7 copy-start.5
